TPU v7x, 32 devices: a whole 2x2x4 slice. The times are simulated.
32 devices in a mesh: grp: 2 (over y), ra: 4 (over z), cb: 2 (over x), dp: 2 (over core).
Axes of the slice: x: 2, y: 2, z: 4, core: 2. Of those that a mesh axis runs over, the one named last changes fastest.
Arguments:
- tokens: bfloat16 [256, 2048], P(('grp', 'dp'), 'ra'), parts along dimension 0, may hold values from -51 to 51
- first_gain: float32 [2048], P('ra'), may hold values from 0.1 to 1.9
- first_gate: float32 [2048, 5632], P('ra', 'cb'), may hold values from -0.125 to 0.125
- first_up: float32 [2048, 5632], P('ra', 'cb'), may hold values from -0.125 to 0.125
- first_down: float32 [5632, 2048], P('cb', 'ra'), may hold values from -0.078125 to 0.078125
- first_gate_scale: float32 [5632], P('cb'), may hold values from 0.1 to 1.9
- first_up_scale: float32 [5632], P('cb'), may hold values from 0.1 to 1.9
- first_down_scale: float32 [2048], P('ra'), may hold values from 0.1 to 1.9
- second_gain: float32 [2048], P('ra'), may hold values from 0.1 to 1.9
- second_gate: float32 [2048, 5632], P('ra', 'cb'), may hold values from -0.125 to 0.125
- second_up: float32 [2048, 5632], P('ra', 'cb'), may hold values from -0.125 to 0.125
- second_down: float32 [5632, 2048], P('cb', 'ra'), may hold values from -0.078125 to 0.078125
- second_gate_scale: float32 [5632], P('cb'), may hold values from 0.1 to 1.9
- second_up_scale: float32 [5632], P('cb'), may hold values from 0.1 to 1.9
- second_down_scale: float32 [2048], P('ra'), may hold values from 0.1 to 1.9
Outputs:
- result: bfloat16 [256, 2048], P(('grp', 'dp'), 'ra'), parts along dimension 0
There are 2 independent parts, one for each index of `grp`. A program takes and returns all parts, laid end to end along the dimension named above; an argument that names none is the same for every part. Nothing has to cross between parts.
All inputs are finite; a program needn't handle non-finite values.
Results may differ from a plain program's by a relative error of at most 0.04.
Values may be sent and summed in bfloat16 or wider, within the bound.
A program may use at most 64 MiB of HBM per device.

v0:
```python
import functools

import jax
import jax.numpy as jnp
from jax import lax
from jax.experimental import pallas as pl
from jax.experimental.pallas import tpu as pltpu
from jax.sharding import PartitionSpec as P

EPS = 1e-06
MESH = pl.DeviceIdType.MESH
LANES = 128
LAG_SUM = 5
LAG_HID = 8


def kernel(dims, *refs):
    n, m, rows, width, units, total_width = dims
    (tokens, gain0, gate0, up0, down0, gs0, us0, ds0, gain1, gate1, up1, down1, gs1, us1, ds1) = refs[:15]
    out = refs[15]
    (values, scaled, gains, dscales, gscales, uscales, w_gu, w_down, own, sum_out, sum_in, cross_in, hid, acc,
     down_in, squares, inverse, small_sem, gate_sem, up_sem, down_sem, sum_ss, sum_rs, cross_rs, hid_ss, hid_rs,
     part_ss, part_rs, sq_ss, sq_rs) = refs[16:]
    gate, up, down = (gate0, gate1), (up0, up1), (down0, down1)
    bf16, f32 = jnp.bfloat16, jnp.float32

    z, x = lax.axis_index("ra"), lax.axis_index("cb")
    blocks = units // LANES
    half = n // 2
    owners = (half - 1, half)
    counts = (blocks - blocks // 2, blocks // 2)
    starts = (0, counts[0])
    left = z < half
    step = jnp.where(left, 1, -1)
    p = jnp.where(left, z, n - 1 - z)
    middle = (z == half - 1) | (z == half)
    first = jnp.where(left, counts[0], 0)
    n_far = jnp.where(left, counts[1], counts[0])
    depth = (half - 1, n - half - 1)
    slots = max(blocks + blocks // 2, blocks + LAG_SUM * max(depth) + LAG_HID)

    def copy_small():
        found = []
        for i, (src, dst) in enumerate((
            (tokens, values), (gain0, gains.at[0]), (gs0, gscales.at[0]), (us0, uscales.at[0]), (ds0, dscales.at[0]),
            (gain1, gains.at[1]), (gs1, gscales.at[1]), (us1, uscales.at[1]), (ds1, dscales.at[1]),
        )):
            found.append(pltpu.make_async_copy(src, dst, small_sem.at[i]))
        return found

    def columns(c):
        return pl.ds(pl.multiple_of(c * LANES, LANES), LANES)

    def gate_copy(l, c):
        return pltpu.make_async_copy(gate[l].at[:, columns(c)], w_gu.at[l, c, :, pl.ds(0, LANES)], gate_sem.at[l, c])

    def up_copy(l, c):
        return pltpu.make_async_copy(up[l].at[:, columns(c)], w_gu.at[l, c, :, pl.ds(LANES, LANES)], up_sem.at[l, c])

    def down_copy(l, c):
        return pltpu.make_async_copy(down[l].at[columns(c), :], w_down.at[l, c], down_sem.at[l, c])

    def sum_copy(l, c):
        return pltpu.make_async_remote_copy(
            src_ref=sum_out.at[l, c], dst_ref=sum_in.at[l, c], send_sem=sum_ss.at[l, c], recv_sem=sum_rs.at[l, c],
            device_id={"ra": z + step}, device_id_type=MESH)

    def cross_copy(l, c):
        return pltpu.make_async_remote_copy(
            src_ref=sum_out.at[l, c], dst_ref=cross_in.at[l, c], send_sem=sum_ss.at[l, c],
            recv_sem=cross_rs.at[l, c], device_id={"ra": z + step}, device_id_type=MESH)

    def hid_copy(l, c, o):
        return pltpu.make_async_remote_copy(
            src_ref=hid.at[l, c], dst_ref=hid.at[l, c], send_sem=hid_ss.at[l, o, c], recv_sem=hid_rs.at[l, c],
            device_id={"ra": lax.rem(z + o, n)}, device_id_type=MESH)

    def part_copy(l, o, sender):
        return pltpu.make_async_remote_copy(
            src_ref=down_in.at[l, sender], dst_ref=down_in.at[l, sender], send_sem=part_ss.at[l, o],
            recv_sem=part_rs.at[l, sender], device_id={"cb": lax.rem(x + o, m)}, device_id_type=MESH)

    def sq_copy(l, end, sender):
        return pltpu.make_async_remote_copy(
            src_ref=squares.at[l, sender], dst_ref=squares.at[l, sender], send_sem=sq_ss.at[l, end],
            recv_sem=sq_rs.at[l, sender], device_id={"ra": owners[end]}, device_id_type=MESH)

    def stream(j):
        return lax.rem(first + j, blocks)

    small = copy_small()
    for copy in small:
        copy.start()

    def start_first(i, carry):
        c = stream(i)
        gate_copy(0, c).start()
        up_copy(0, c).start()
        return carry

    lax.fori_loop(0, blocks, start_first, 0)

    barrier = pltpu.get_barrier_semaphore()
    for o in range(1, n):
        pl.semaphore_signal(barrier, inc=1, device_id={"ra": lax.rem(z + o, n)}, device_id_type=MESH)
    for o in range(1, m):
        pl.semaphore_signal(barrier, inc=1, device_id={"cb": lax.rem(x + o, m)}, device_id_type=MESH)
    for copy in small:
        copy.wait()

    for l in range(2):
        floats = values[...].astype(f32)
        scaled[...] = (floats * gains[l]).astype(bf16)
        squares[l, z] = lax.dot_general(
            jnp.ones((8, width), f32), floats * floats, (((1,), (1,)), ((), ())),
            precision=lax.Precision.HIGHEST, preferred_element_type=f32)
        acc[...] = jnp.zeros_like(acc)
        if l == 0:
            pl.semaphore_wait(barrier, n + m - 2)
        for end in range(2):
            @pl.when(z != owners[end])
            def _():
                sq_copy(l, end, z).start()

        def use_hidden(c, block):
            down_copy(l, c).wait()
            acc[...] += jnp.dot(block, w_down[l, c].astype(bf16), preferred_element_type=f32)

        def slot(s, carry):
            if l == 0:
                @pl.when(s < blocks)
                def _():
                    down_copy(0, stream(s)).start()

                later = s - blocks // 2

                @pl.when((later >= 0) & (later < blocks))
                def _():
                    c = stream(later)
                    gate_copy(1, c).start()
                    up_copy(1, c).start()
                    down_copy(1, c).start()

            @pl.when(s < blocks)
            def _():
                c = stream(s)
                gate_copy(l, c).wait()
                up_copy(l, c).wait()
                own[c] = jnp.dot(scaled[...], w_gu[l, c].astype(bf16), preferred_element_type=f32)

            k = s - LAG_SUM * p
            c = stream(jnp.clip(k, 0, blocks - 1))
            turn = (k >= 0) & (k < blocks)
            mine = middle & (k >= n_far)

            @pl.when(turn & jnp.logical_not(mine))
            def _():
                @pl.when(p == 0)
                def _():
                    sum_out[l, c] = own[c].astype(bf16)

                @pl.when(p > 0)
                def _():
                    sum_copy(l, c).wait_recv()
                    sum_out[l, c] = (own[c] + sum_in[l, c].astype(f32)).astype(bf16)

                @pl.when(middle)
                def _():
                    cross_copy(l, c).start()

                @pl.when(jnp.logical_not(middle))
                def _():
                    sum_copy(l, c).start()

            @pl.when(turn & mine)
            def _():
                @pl.when(k == n_far)
                def _():
                    for o in range(1, n):
                        sq_copy(l, 0, lax.rem(z + o, n)).wait_recv()
                    every = squares[l].reshape(8 * n, rows)
                    total = lax.dot_general(
                        every, jnp.full((8 * n, LANES), 0.125, f32), (((0,), (0,)), ((), ())),
                        precision=lax.Precision.HIGHEST, preferred_element_type=f32)
                    inverse[...] = lax.rsqrt(total / total_width + EPS)

                @pl.when(p > 0)
                def _():
                    sum_copy(l, c).wait_recv()
                    own[c] += sum_in[l, c].astype(f32)

                cross_copy(l, c).wait_recv()
                both = own[c] + cross_in[l, c].astype(f32)
                inv = inverse[...]
                g = both[:, :LANES] * gscales[l, pl.ds(c, 1), :] * inv
                u = both[:, LANES:] * uscales[l, pl.ds(c, 1), :] * inv
                block = (g / (1.0 + jnp.exp(-g)) * u).astype(bf16)
                hid[l, c] = block
                for o in range(1, n):
                    hid_copy(l, c, o).start()
                use_hidden(c, block)

            for d in range(2):
                k2 = s - counts[1 - d] - LAG_SUM * depth[d] - LAG_HID

                @pl.when((k2 >= 0) & (k2 < counts[d]) & (z != owners[d]))
                def _():
                    c2 = starts[d] + k2
                    hid_copy(l, c2, 1).wait_recv()
                    use_hidden(c2, hid[l, c2])
            return carry

        lax.fori_loop(0, slots, slot, 0)

        down_in[l, x] = acc[...].astype(bf16)
        for o in range(1, m):
            part_copy(l, o, x).start()
        for o in range(1, m):
            part_copy(l, o, lax.rem(x + o, m)).wait_recv()
        total = down_in[l, 0].astype(f32)
        for o in range(1, m):
            total = total + down_in[l, o].astype(f32)
        result = (0.3 * values[...].astype(f32) + 0.5 * total * dscales[l]).astype(bf16)
        if l == 0:
            values[...] = result
        else:
            out[...] = result

    for l in range(2):
        for o in range(1, m):
            part_copy(l, o, x).wait_send()
        for end in range(2):
            @pl.when(z != owners[end])
            def _():
                sq_copy(l, end, z).wait_send()
        def sent_sum(k, carry):
            sum_copy(l, stream(k)).wait_send()
            return carry

        lax.fori_loop(0, jnp.where(middle, n_far, blocks), sent_sum, 0)

        @pl.when(middle)
        def _():
            def sent_hid(k, carry):
                for o in range(1, n):
                    hid_copy(l, stream(n_far + k), o).wait_send()
                return carry
            lax.fori_loop(0, blocks - n_far, sent_hid, 0)


def per_device(n, m, *args):
    tokens = args[0]
    rows, width = tokens.shape
    units = args[2].shape[1]
    blocks = units // LANES
    bf16, f32 = jnp.bfloat16, jnp.float32
    flat = [a if a.ndim > 1 else a.reshape(1, width) if i in (1, 7, 8, 14) else a.reshape(blocks, LANES) for i, a in enumerate(args)]
    dma = pltpu.SemaphoreType.DMA
    return pl.pallas_call(
        functools.partial(kernel, (n, m, rows, width, units, n * width)),
        out_shape=jax.ShapeDtypeStruct((rows, width), bf16),
        in_specs=[pl.BlockSpec(memory_space=pl.ANY)] * len(flat),
        out_specs=pl.BlockSpec(memory_space=pltpu.VMEM),
        scratch_shapes=[
            pltpu.VMEM((rows, width), bf16),
            pltpu.VMEM((rows, width), bf16),
            pltpu.VMEM((2, 1, width), f32),
            pltpu.VMEM((2, 1, width), f32),
            pltpu.VMEM((2, blocks, LANES), f32),
            pltpu.VMEM((2, blocks, LANES), f32),
            pltpu.VMEM((2, blocks, width, 2 * LANES), f32),
            pltpu.VMEM((2, blocks, LANES, width), f32),
            pltpu.VMEM((blocks, rows, 2 * LANES), f32),
            pltpu.VMEM((2, blocks, rows, 2 * LANES), bf16),
            pltpu.VMEM((2, blocks, rows, 2 * LANES), bf16),
            pltpu.VMEM((2, blocks, rows, 2 * LANES), bf16),
            pltpu.VMEM((2, blocks, rows, LANES), bf16),
            pltpu.VMEM((rows, width), f32),
            pltpu.VMEM((2, m, rows, width), bf16),
            pltpu.VMEM((2, n, 8, rows), f32),
            pltpu.VMEM((rows, LANES), f32),
            dma((9,)),
            dma((2, blocks)),
            dma((2, blocks)),
            dma((2, blocks)),
            dma((2, blocks)),
            dma((2, blocks)),
            dma((2, blocks)),
            dma((2, n, blocks)),
            dma((2, blocks)),
            dma((2, m)),
            dma((2, m)),
            dma((2, 2)),
            dma((2, n)),
        ],
        compiler_params=pltpu.CompilerParams(
            collective_id=0, has_side_effects=True, vmem_limit_bytes=60 * 1024 * 1024
        ),
    )(*flat)


def solution(mesh):
    in_specs = (
        P(("grp", "dp"), "ra"),
        P("ra"),
        P("ra", "cb"),
        P("ra", "cb"),
        P("cb", "ra"),
        P("cb"),
        P("cb"),
        P("ra"),
        P("ra"),
        P("ra", "cb"),
        P("ra", "cb"),
        P("cb", "ra"),
        P("cb"),
        P("cb"),
        P("ra"),
    )
    out_specs = P(("grp", "dp"), "ra")
    n, m = mesh.shape["ra"], mesh.shape["cb"]
    return jax.shard_map(
        functools.partial(per_device, n, m), mesh=mesh, in_specs=in_specs, out_specs=out_specs, check_vma=False
    )
```

profile of v0, /device:TPU:0, one launch (start us, length us, event | category | flops | bytes accessed | tf_op | source)
XLA Modules:
  0.0 59.5 jit_solution(4634393250569619335)
XLA Ops:
  0.0 58.0 %shard_map.145 = bf16[64,512]{1,0:T(8,128)(2,1)} custom-call(bf16[64,512]{1,0:T(8,128)(2,1)} %refs_0_.1, f32[1,512]{1,0:T(1,128)} %bitcast.12, f32[512,2816]{1,0:T(8,128)} %refs_2_.1, f32[512,2816]{1,0:T(8,128)} %refs_3_.1, f32[2816,512]{1,0:T(8,128)} %refs_4_.1, f32[22,128]{1,0:T(8,128)} %bitcast.8, f32[22,128]{1,0:T(8,128)} %bitcast.9, f32[1,512]{1,0:T(1,128)} %bitcast.13, ...), custom_call_target="tpu_custom_call" | custom-call | tf_op jit(solution)/shard_map/pallas_call | solution.py:259
  58.0 1.5 %copy.17 = bf16[64,512]{1,0:T(8,128)(2,1)} copy(bf16[64,512]{1,0:T(8,128)(2,1)} %shard_map.145) | data formatting | bytes 131072
where the time goes:
time: 59.6 us; the launch traced here: 59.5 us
  Pallas kernels  58 us (97%)
  local copies, waits for them, and re-layouts  1.47 us (2%)
    pallas_call x1, Pallas kernels, per_device(): pl.pallas_call(functools.partial(kernel, (n, m, rows, width, units, n * w...  58 us
    unnamed x1, local copies, waits for them, and re-layouts  1.47 us

commit v1 on v0

v1 whole, which is shorter than its diff:
```python
import functools

import jax
import jax.numpy as jnp
from jax import lax
from jax.experimental import pallas as pl
from jax.experimental.pallas import tpu as pltpu
from jax.sharding import PartitionSpec as P

EPS = 1e-06
MESH = pl.DeviceIdType.MESH
LANES = 128
LAG = 5


def kernel(dims, *refs):
    n, m, cores, rows, width, units, pieces, total_width = dims
    (tokens, gain0, gate0, up0, down0, gs0, us0, ds0, gain1, gate1, up1, down1, gs1, us1, ds1) = refs[:15]
    out = refs[15]
    (values, scaled, vectors, scales, w_gu, w_down, own, sum_out, sum_in, cross_in, hid, acc, down_in, squares, inverse,
     small_sem, gu_sem, down_sem, sum_ss, sum_rs, cross_rs, hid_ss, hid_rs, part_ss, part_rs, sq_ss, sq_rs,
     turn_sem) = refs[16:]
    gate, up, down = (gate0, gate1), (up0, up1), (down0, down1)
    bf16, f32 = jnp.bfloat16, jnp.float32
    scope = jax.named_scope

    z, x, core = lax.axis_index("ra"), lax.axis_index("cb"), lax.axis_index("dp")
    lanes = pieces * LANES
    blocks = units // lanes
    half = n // 2
    owners = (half - 1, half)
    counts = (blocks - blocks // 2, blocks // 2)
    starts = (0, counts[0])
    left = z < half
    step = jnp.where(left, 1, -1)
    p = jnp.where(left, z, n - 1 - z)
    middle = (z == half - 1) | (z == half)
    first = jnp.where(left, counts[0], 0)
    n_far = jnp.where(left, counts[1], counts[0])
    n_near = blocks - n_far
    near_start = jnp.where(left, 0, counts[0])

    def wait(ref, sem):
        pltpu.make_async_copy(ref, ref, sem).wait()

    def columns(c):
        return pl.ds(pl.multiple_of(c * lanes, lanes), lanes)

    def gate_copy(l, c):
        return pltpu.make_async_copy(gate[l].at[:, columns(c)], w_gu.at[l, c, :, pl.ds(0, lanes)], gu_sem.at[c])

    def up_copy(l, c):
        return pltpu.make_async_copy(up[l].at[:, columns(c)], w_gu.at[l, c, :, pl.ds(lanes, lanes)], gu_sem.at[c])

    def down_copy(l, c):
        return pltpu.make_async_copy(down[l].at[columns(c), :], w_down.at[l, c], down_sem.at[c])

    def sum_copy(l, b):
        return pltpu.make_async_remote_copy(
            src_ref=sum_out.at[l, b], dst_ref=sum_in.at[l, b], send_sem=sum_ss.at[l], recv_sem=sum_rs.at[b],
            device_id={"ra": z + step}, device_id_type=MESH)

    def cross_copy(l, b):
        return pltpu.make_async_remote_copy(
            src_ref=sum_out.at[l, b], dst_ref=cross_in.at[l, b], send_sem=sum_ss.at[l],
            recv_sem=cross_rs.at[b - first * pieces], device_id={"ra": z + step}, device_id_type=MESH)

    def hid_copy(l, c, i, dest):
        part = hid.at[l, c, :, pl.ds(i * LANES, LANES)]
        return pltpu.make_async_remote_copy(
            src_ref=part, dst_ref=part, send_sem=hid_ss.at[l, dest], recv_sem=hid_rs.at[c],
            device_id={"ra": dest}, device_id_type=MESH)

    def part_copy(l, o, sender):
        return pltpu.make_async_remote_copy(
            src_ref=down_in.at[l, sender], dst_ref=down_in.at[l, sender], send_sem=part_ss.at[l, o],
            recv_sem=part_rs.at[l, sender], device_id={"cb": lax.rem(x + o, m)}, device_id_type=MESH)

    def sq_copy(l, end, sender):
        return pltpu.make_async_remote_copy(
            src_ref=squares.at[l, sender], dst_ref=squares.at[l, sender], send_sem=sq_ss.at[l, end],
            recv_sem=sq_rs, device_id={"ra": owners[end]}, device_id_type=MESH)

    def others():
        return [jnp.where(left, n - 1 - o, o) + jnp.where(
            left, jnp.where(n - 1 - o <= z, -1, 0), jnp.where(o >= z, 1, 0)) for o in range(n - 1)]

    def stream(j):
        return lax.rem(first + j, blocks)

    def loop(low, high, step_fn):
        def one(i, carry):
            step_fn(i)
            return carry
        lax.fori_loop(low, high, one, 0)

    urgent = [pltpu.make_async_copy(tokens, values, small_sem.at[0]),
              pltpu.make_async_copy(gain0, vectors.at[3], small_sem.at[1])]
    for copy in urgent:
        copy.start()

    def start_first(i):
        c = stream(i)
        gate_copy(0, c).start()
        up_copy(0, c).start()

    loop(0, blocks, start_first)
    for i, src in enumerate((ds0, gain1, ds1)):
        pltpu.make_async_copy(src, vectors.at[i], small_sem.at[2]).start()
    for i, src in enumerate((gs0, gs1, us0, us1)):
        pltpu.make_async_copy(src, scales.at[i], small_sem.at[3]).start()

    barrier = pltpu.get_barrier_semaphore()

    def greet(device):
        pl.semaphore_signal(barrier, inc=1, device_id={"ra": device}, device_id_type=MESH)

    @pl.when(middle)
    def _():
        for o in range(1, n):
            greet(lax.rem(z + o, n))

    @pl.when(jnp.logical_not(middle))
    def _():
        for owner in owners:
            greet(owner)

        @pl.when(p < half - 2)
        def _():
            greet(z + step)

        @pl.when(p > 0)
        def _():
            greet(z - step)

    for o in range(1, m):
        pl.semaphore_signal(barrier, inc=1, device_id={"cb": lax.rem(x + o, m)}, device_id_type=MESH)
    for o in range(1, cores):
        pl.semaphore_signal(barrier, inc=1, device_id={"dp": lax.rem(core + o, cores)}, device_id_type=MESH)
    with scope("small"):
        for copy in urgent:
            copy.wait()

    for l in range(2):
        scaled[...] = (values[...].astype(f32) * vectors[(3, 1)[l]]).astype(bf16)
        if l == 0:
            with scope("barrier"):
                greeted = jnp.where(middle, n - 1, 2 + jnp.where(p < half - 2, 1, 0) + jnp.where(p > 0, 1, 0))
                pl.semaphore_wait(barrier, greeted + m + cores - 2)

        def product(k, store):
            if l == 0:
                down_copy(0, stream(k)).start()
            c = stream(k)
            with scope("w_gu"):
                wait(w_gu.at[l, c], gu_sem.at[c])
            both = jnp.dot(scaled[...], w_gu[l, c].astype(bf16), preferred_element_type=f32)
            for i in range(pieces):
                a, b = i * LANES, lanes + i * LANES
                store(c * pieces + i, both[:, a:a + LANES], both[:, b:b + LANES])

        def send_squares(k):
            @pl.when(k == 1)
            def _():
                floats = values[...].astype(f32)
                squares[l, z] = lax.dot_general(
                    jnp.ones((8, width), f32), floats * floats, (((1,), (1,)), ((), ())),
                    precision=lax.Precision.HIGHEST, preferred_element_type=f32)
                for end in range(2):
                    @pl.when(z != owners[end])
                    def _():
                        sq_copy(l, end, z).start()

        def fetch_second():
            if l == 0:
                def one(k):
                    c = stream(k)
                    gate_copy(1, c).start()
                    up_copy(1, c).start()
                loop(0, blocks, one)

        def use_hidden(c):
            with scope("w_down"):
                down_copy(l, c).wait()
            acc[...] += jnp.dot(hid[l, c], w_down[l, c].astype(bf16), preferred_element_type=f32)

        def wait_hidden(c):
            with scope("w_hid"):
                wait(hid.at[l, c], hid_rs.at[c])

        def to_out(b, g, u):
            sum_out[l, b, :, :LANES] = g.astype(bf16)
            sum_out[l, b, :, LANES:] = u.astype(bf16)

        def to_own(b, g, u):
            own[b, :, :LANES] = g
            own[b, :, LANES:] = u

        def pass_on(b, copy):
            with scope("w_sum"):
                sum_copy(l, b).wait_recv()
            sum_out[l, b] = (own[b] + sum_in[l, b].astype(f32)).astype(bf16)
            copy(l, b).start()

        @pl.when(jnp.logical_not(middle))
        def _():
            @pl.when(p == 0)
            def _():
                def make(k):
                    product(k, to_out)
                    send = [sum_copy(l, stream(k) * pieces + i) for i in range(pieces)]
                    if l == 0:
                        @pl.when(core == 0)
                        def _():
                            for copy in send:
                                copy.start()
                    else:
                        for copy in send:
                            copy.start()
                    send_squares(k)

                with scope("make"):
                    loop(0, blocks, make)
                fetch_second()
                if l == 0:
                    @pl.when(core > 0)
                    def _():
                        with scope("turn"):
                            pl.semaphore_wait(turn_sem, 1)

                        def one(k):
                            for i in range(pieces):
                                sum_copy(l, stream(k) * pieces + i).start()
                        loop(0, blocks, one)

                    @pl.when(core < cores - 1)
                    def _():
                        with scope("held"):
                            wait(sum_out.at[l], sum_ss.at[l])
                        pl.semaphore_signal(turn_sem, inc=1, device_id={"dp": core + 1}, device_id_type=MESH)

            @pl.when(p > 0)
            def _():
                def relay(k):
                    product(k, to_own)
                    send_squares(k)
                    for i in range(pieces):
                        pass_on(stream(k) * pieces + i, sum_copy)

                loop(0, blocks, relay)
                fetch_second()

            acc[...] = jnp.zeros_like(acc)

            def gather(k):
                for d in range(2):
                    @pl.when(k < counts[d])
                    def _():
                        wait_hidden(starts[d] + k)
                        use_hidden(starts[d] + k)

            with scope("gather"):
                loop(0, counts[0], gather)

        @pl.when(middle)
        def _():
            ahead = blocks // 2

            def make(k):
                product(k, to_own)
                send_squares(k)

            with scope("make"):
                loop(0, ahead, make)

            def far(k):
                make(k)

                @pl.when(k - ahead < n_far)
                def _():
                    for i in range(pieces):
                        b = stream(k - ahead) * pieces + i
                        if half == 1:
                            sum_out[l, b] = own[b].astype(bf16)
                            cross_copy(l, b).start()
                        else:
                            pass_on(b, cross_copy)

            with scope("far"):
                loop(ahead, blocks, far)
            fetch_second()
            acc[...] = jnp.zeros_like(acc)
            with scope("w_sq"):
                wait(squares.at[l, pl.ds(0, n - 1)], sq_rs)
            every = squares[l].reshape(8 * n, rows)
            total = lax.dot_general(
                every, jnp.full((8 * n, LANES), 0.125, f32), (((0,), (0,)), ((), ())),
                precision=lax.Precision.HIGHEST, preferred_element_type=f32)
            inverse[...] = lax.rsqrt(total / total_width + EPS)
            if l == 0:
                with scope("w_small"):
                    wait(scales, small_sem.at[3])

            def near(s):
                @pl.when(s < n_near)
                def _():
                    c = near_start + s
                    for i in range(pieces):
                        b = c * pieces + i
                        both = own[b]
                        if half > 1:
                            with scope("w_sum"):
                                sum_copy(l, b).wait_recv()
                            both = both + sum_in[l, b].astype(f32)
                        with scope("w_cross"):
                            wait(cross_in.at[l, b], cross_rs.at[b - near_start * pieces])
                        both = both + cross_in[l, b].astype(f32)
                        inv = inverse[...]
                        g = both[:, :LANES] * scales[l, pl.ds(b, 1), :] * inv
                        u = both[:, LANES:] * scales[2 + l, pl.ds(b, 1), :] * inv
                        hid[l, c, :, i * LANES:(i + 1) * LANES] = (g / (1.0 + jnp.exp(-g)) * u).astype(bf16)
                        for dest in others():
                            hid_copy(l, c, i, dest).start()
                    use_hidden(c)

                k = s - LAG

                @pl.when((k >= 0) & (k < n_far))
                def _():
                    wait_hidden(first + k)
                    use_hidden(first + k)

            with scope("near"):
                loop(0, counts[0] + LAG, near)

        down_in[l, x] = acc[...].astype(bf16)
        for o in range(1, m):
            part_copy(l, o, x).start()
        if l == 0:
            loop(0, blocks, lambda k: down_copy(1, k).start())
            wait(vectors.at[pl.ds(0, 3)], small_sem.at[2])

            @pl.when(jnp.logical_not(middle))
            def _():
                wait(scales, small_sem.at[3])
        with scope("exch"):
            for o in range(1, m):
                part_copy(l, o, lax.rem(x + o, m)).wait_recv()
        total = down_in[l, 0].astype(f32)
        for o in range(1, m):
            total = total + down_in[l, o].astype(f32)
        result = (0.3 * values[...].astype(f32) + 0.5 * total * vectors[(0, 2)[l]]).astype(bf16)
        if l == 0:
            values[...] = result
        else:
            out[...] = result

    with scope("drain"):
        for l in range(2):
            for o in range(1, m):
                part_copy(l, o, x).wait_send()
            for end in range(2):
                @pl.when(z != owners[end])
                def _():
                    sq_copy(l, end, z).wait_send()

            kept = core == cores - 1 if l == 0 else True

            @pl.when(jnp.logical_not(middle) & (kept | (p > 0)))
            def _():
                wait(sum_out.at[l], sum_ss.at[l])

            for d in range(2):
                @pl.when(z == owners[d])
                def _():
                    wait(sum_out.at[l, pl.ds(0, counts[1 - d] * pieces)], sum_ss.at[l])
                    for dest in range(n):
                        if dest != owners[d]:
                            wait(hid.at[l, pl.ds(0, counts[d])], hid_ss.at[l, dest])


def per_device(n, m, cores, *args):
    tokens = args[0]
    rows, width = tokens.shape
    units = args[2].shape[1]
    pieces = 2 if units % (2 * LANES) == 0 else 1
    lanes = pieces * LANES
    blocks = units // lanes
    parts = units // LANES
    bf16, f32 = jnp.bfloat16, jnp.float32
    flat = [a if a.ndim > 1 else a.reshape(1, width) if i in (1, 7, 8, 14) else a.reshape(parts, LANES) for i, a in enumerate(args)]
    dma = pltpu.SemaphoreType.DMA
    return pl.pallas_call(
        functools.partial(kernel, (n, m, cores, rows, width, units, pieces, n * width)),
        out_shape=jax.ShapeDtypeStruct((rows, width), bf16),
        in_specs=[pl.BlockSpec(memory_space=pl.ANY)] * len(flat),
        out_specs=pl.BlockSpec(memory_space=pltpu.VMEM),
        scratch_shapes=[
            pltpu.VMEM((rows, width), bf16),
            pltpu.VMEM((rows, width), bf16),
            pltpu.VMEM((4, 1, width), f32),
            pltpu.VMEM((4, parts, LANES), f32),
            pltpu.VMEM((2, blocks, width, 2 * lanes), f32),
            pltpu.VMEM((2, blocks, lanes, width), f32),
            pltpu.VMEM((parts, rows, 2 * LANES), f32),
            pltpu.VMEM((2, parts, rows, 2 * LANES), bf16),
            pltpu.VMEM((2, parts, rows, 2 * LANES), bf16),
            pltpu.VMEM((2, parts, rows, 2 * LANES), bf16),
            pltpu.VMEM((2, blocks, rows, lanes), bf16),
            pltpu.VMEM((rows, width), f32),
            pltpu.VMEM((2, m, rows, width), bf16),
            pltpu.VMEM((2, n, 8, rows), f32),
            pltpu.VMEM((rows, LANES), f32),
            dma((4,)),
            dma((blocks,)),
            dma((blocks,)),
            dma((2,)),
            dma((parts,)),
            dma(((blocks - blocks // 2) * pieces,)),
            dma((2, n)),
            dma((blocks,)),
            dma((2, m)),
            dma((2, m)),
            dma((2, 2)),
            dma,
            pltpu.SemaphoreType.REGULAR,
        ],
        compiler_params=pltpu.CompilerParams(
            collective_id=0, has_side_effects=True, vmem_limit_bytes=60 * 1024 * 1024
        ),
    )(*flat)


def solution(mesh):
    in_specs = (
        P(("grp", "dp"), "ra"),
        P("ra"),
        P("ra", "cb"),
        P("ra", "cb"),
        P("cb", "ra"),
        P("cb"),
        P("cb"),
        P("ra"),
        P("ra"),
        P("ra", "cb"),
        P("ra", "cb"),
        P("cb", "ra"),
        P("cb"),
        P("cb"),
        P("ra"),
    )
    out_specs = P(("grp", "dp"), "ra")
    n, m, cores = mesh.shape["ra"], mesh.shape["cb"], mesh.shape["dp"]
    return jax.shard_map(
        functools.partial(per_device, n, m, cores), mesh=mesh, in_specs=in_specs, out_specs=out_specs, check_vma=False
    )
```

time: 59.6 us -> 49 us (0.82)
  the two profiles are of different devices: /device:TPU:0 before, /device:TPU:1 now
where the time goes in v1:
time: 49 us; the launch traced here: 48.8 us
  Pallas kernels  47.3 us (97%)
  local copies, waits for them, and re-layouts  1.47 us (3%)
    pallas_call x1, Pallas kernels, per_device(): pl.pallas_call(functools.partial(kernel, (n, m, cores, rows, width, units...  47.3 us
    unnamed x1, local copies, waits for them, and re-layouts  1.47 us

profile of v1, /device:TPU:1, one launch (start us, length us, event | category | flops | bytes accessed | tf_op | source)
XLA Modules:
  0.0 48.8 jit_solution(9553902706307420795)
XLA Ops:
  0.0 47.3 %shard_map.145 = bf16[64,512]{1,0:T(8,128)(2,1)} custom-call(bf16[64,512]{1,0:T(8,128)(2,1)} %refs_0_.1, f32[1,512]{1,0:T(1,128)} %bitcast.12, f32[512,2816]{1,0:T(8,128)} %refs_2_.1, f32[512,2816]{1,0:T(8,128)} %refs_3_.1, f32[2816,512]{1,0:T(8,128)} %refs_4_.1, f32[22,128]{1,0:T(8,128)} %bitcast.8, f32[22,128]{1,0:T(8,128)} %bitcast.9, f32[1,512]{1,0:T(1,128)} %bitcast.13, ...), custom_call_target="tpu_custom_call" | custom-call | tf_op jit(solution)/shard_map/pallas_call | solution.py:393
  47.3 1.5 %copy.17 = bf16[64,512]{1,0:T(8,128)(2,1)} copy(bf16[64,512]{1,0:T(8,128)(2,1)} %shard_map.145) | data formatting | bytes 131072

commit v2 on v1

--- a/solution.py
+++ b/solution.py
@@ -73,12 +73,12 @@
 
     def part_copy(l, o, sender):
         return pltpu.make_async_remote_copy(
-            src_ref=down_in.at[l, sender], dst_ref=down_in.at[l, sender], send_sem=part_ss.at[l, o],
-            recv_sem=part_rs.at[l, sender], device_id={"cb": lax.rem(x + o, m)}, device_id_type=MESH)
+            src_ref=down_in.at[l, sender], dst_ref=down_in.at[l, sender], send_sem=part_ss.at[l, o - 1],
+            recv_sem=part_rs.at[l, o - 1], device_id={"cb": lax.rem(x + o, m)}, device_id_type=MESH)
 
     def sq_copy(l, end, sender):
         return pltpu.make_async_remote_copy(
-            src_ref=squares.at[l, sender], dst_ref=squares.at[l, sender], send_sem=sq_ss.at[l, end],
+            src_ref=squares.at[l, sender], dst_ref=squares.at[l, sender], send_sem=sq_ss.at[l],
             recv_sem=sq_rs, device_id={"ra": owners[end]}, device_id_type=MESH)
 
     def others():
@@ -180,8 +180,7 @@
                 loop(0, blocks, one)
 
         def use_hidden(c):
-            with scope("w_down"):
-                down_copy(l, c).wait()
+            down_copy(l, c).wait()
             acc[...] += jnp.dot(hid[l, c], w_down[l, c].astype(bf16), preferred_element_type=f32)
 
         def wait_hidden(c):
@@ -345,7 +344,7 @@
                 wait(scales, small_sem.at[3])
         with scope("exch"):
             for o in range(1, m):
-                part_copy(l, o, lax.rem(x + o, m)).wait_recv()
+                part_copy(l, o, lax.rem(x - o + m, m)).wait_recv()
         total = down_in[l, 0].astype(f32)
         for o in range(1, m):
             total = total + down_in[l, o].astype(f32)
@@ -359,20 +358,20 @@
         for l in range(2):
             for o in range(1, m):
                 part_copy(l, o, x).wait_send()
-            for end in range(2):
-                @pl.when(z != owners[end])
-                def _():
-                    sq_copy(l, end, z).wait_send()
-
             kept = core == cores - 1 if l == 0 else True
 
             @pl.when(jnp.logical_not(middle) & (kept | (p > 0)))
             def _():
                 wait(sum_out.at[l], sum_ss.at[l])
+
+            @pl.when(jnp.logical_not(middle))
+            def _():
+                wait(squares.at[l, pl.ds(0, 2)], sq_ss.at[l])
 
             for d in range(2):
                 @pl.when(z == owners[d])
                 def _():
+                    wait(squares.at[l, 0], sq_ss.at[l])
                     wait(sum_out.at[l, pl.ds(0, counts[1 - d] * pieces)], sum_ss.at[l])
                     for dest in range(n):
                         if dest != owners[d]:
@@ -392,7 +391,7 @@
     dma = pltpu.SemaphoreType.DMA
     return pl.pallas_call(
         functools.partial(kernel, (n, m, cores, rows, width, units, pieces, n * width)),
-        out_shape=jax.ShapeDtypeStruct((rows, width), bf16),
+        out_shape=pltpu.VMEM((rows, width), bf16),
         in_specs=[pl.BlockSpec(memory_space=pl.ANY)] * len(flat),
         out_specs=pl.BlockSpec(memory_space=pltpu.VMEM),
         scratch_shapes=[
@@ -419,9 +418,9 @@
             dma(((blocks - blocks // 2) * pieces,)),
             dma((2, n)),
             dma((blocks,)),
-            dma((2, m)),
-            dma((2, m)),
-            dma((2, 2)),
+            dma((2, m - 1)),
+            dma((2, m - 1)),
+            dma((2,)),
             dma,
             pltpu.SemaphoreType.REGULAR,
         ],

time: 49 us -> 47.4 us (0.967)
  local copies, waits for them, and re-layouts: 1.47 us -> 0.63 us
  Pallas kernels: 47.3 us -> 46.6 us
    unnamed x1, local copies, waits for them, and re-layouts: 1.47 us -> 0.63 us
    pallas_call x1, Pallas kernels: 47.3 us -> 46.6 us  [per_device(): pl.pallas_call(functools.partial(kernel, (n, m, cores, rows, width, units...]
where the time goes in v2:
time: 47.4 us; the launch traced here: 47.3 us
  Pallas kernels  46.6 us (98%)
  local copies, waits for them, and re-layouts  0.63 us (1%)
    pallas_call x1, Pallas kernels, per_device(): pl.pallas_call(functools.partial(kernel, (n, m, cores, rows, width, units...  46.6 us

profile of v2, /device:TPU:1, one launch (start us, length us, event | category | flops | bytes accessed | tf_op | source)
XLA Modules:
  0.0 47.3 jit_solution(17187490834245520462)
XLA Ops:
  0.0 46.6 %shard_map.145 = bf16[64,512]{1,0:T(8,128)(2,1)S(1)} custom-call(bf16[64,512]{1,0:T(8,128)(2,1)} %refs_0_.1, f32[1,512]{1,0:T(1,128)} %bitcast.12, f32[512,2816]{1,0:T(8,128)} %refs_2_.1, f32[512,2816]{1,0:T(8,128)} %refs_3_.1, f32[2816,512]{1,0:T(8,128)} %refs_4_.1, f32[22,128]{1,0:T(8,128)} %bitcast.8, f32[22,128]{1,0:T(8,128)} %bitcast.9, ...), custom_call_target="tpu_custom_call" | custom-call | tf_op jit(solution)/shard_map/pallas_call | solution.py:392
  46.6 0.6 %copy.17 = bf16[64,512]{1,0:T(8,128)(2,1)} copy(bf16[64,512]{1,0:T(8,128)(2,1)S(1)} %shard_map.145) | data formatting | bytes 131072
